TPU v7x, 512 devices: a whole 4x8x8 slice. The times are simulated.
512 devices in a mesh: sp: 64 (over z, y), tp: 8 (over x, core).
Axes of the slice: x: 4, y: 8, z: 8, core: 2. Of those that a mesh axis runs over, the one named last changes fastest.
Arguments:
- latent: bfloat16 [16384, 2048], P('sp'), may hold values from -6 to 6
- context: bfloat16 [512, 2048], P('sp'), may hold values from -6 to 6
- cond: bfloat16 [2048], P('sp'), may hold values from -6 to 6
- cond_ctx: bfloat16 [2048], P('sp'), may hold values from -6 to 6
- shift_weight: bfloat16 [2048, 2048], P('sp', 'tp'), may hold values from -0.125 to 0.125
- scale_weight: bfloat16 [2048, 2048], P('sp', 'tp'), may hold values from -0.125 to 0.125
- gate_weight: bfloat16 [2048, 2048], P('sp', 'tp'), may hold values from -0.25 to 0.25
- norm_gain: bfloat16 [2048], replicated, may hold values from 0.099609375 to 1.8984375
- query_weight: bfloat16 [2048, 1024], P(None, 'tp'), may hold values from -0.125 to 0.125
- key_weight: bfloat16 [2048, 1024], P(None, 'tp'), may hold values from -0.125 to 0.125
- value_weight: bfloat16 [2048, 1024], P(None, 'tp'), may hold values from -0.125 to 0.125
- query_gain: bfloat16 [64], replicated, may hold values from 0.099609375 to 1.8984375
- key_gain: bfloat16 [64], replicated, may hold values from 0.099609375 to 1.8984375
- offset_bias: float32 [16, 15, 31], P('tp'), may hold values from -0.5 to 251
- out_weight: bfloat16 [1024, 2048], P(None, 'tp'), may hold values from -1.5 to 1.5
Outputs:
- updated: bfloat16 [16384, 2048], P('sp', 'tp')
All inputs are finite; a program needn't handle non-finite values.
Results may differ from a plain program's by a relative error of at most 0.0077.
Values may be sent and summed in bfloat16 or wider, within the bound.
A program may use at most 64 MiB of HBM per device.

v0:
```python
import jax
import jax.numpy as jnp
import numpy as np
from jax import lax
from jax.sharding import Mesh
from jax.sharding import PartitionSpec as P

HEAD_DIM = 64
WIN_ROWS = 8
WIN_COLS = 16
GRID_W = 64
SP = ("sp_0", "sp_1")
EPS = 1e-06


def one_axis_at_a_time(x, axes):
    for axis in axes:
        x = lax.psum(x, axis)
    return x


def in_order(pieces, dim):
    dims = list(pieces.shape[1:])
    dims[dim] *= pieces.shape[0]
    return jnp.moveaxis(pieces, 0, dim).reshape(dims)


def sent_to_all(x, axis):
    copies = jnp.broadcast_to(x, (lax.axis_size(axis), *x.shape))
    return lax.all_to_all(copies, axis, split_axis=0, concat_axis=0, tiled=True)


def collect(x, axis, dim):
    return in_order(sent_to_all(x, axis), dim)


def side_by_side(arrays, axis, dim, along):
    widths = [a.shape[along] for a in arrays]
    both = jnp.concatenate(arrays, axis=along)
    result = collect(both, axis, dim)
    return tuple(jnp.split(result, [sum(widths[:k]) for k in range(1, len(widths))], axis=along))


def padded_2(block, sides, width):
    for axis, dim in sides:
        count = lax.axis_size(axis)
        forward = [(i, i + 1) for i in range(count - 1)]
        backward = [(target, source) for source, target in forward]
        low = lax.ppermute(
            lax.slice_in_dim(block, block.shape[dim] - width, None, axis=dim), axis, forward
        )
        high = lax.ppermute(lax.slice_in_dim(block, 0, width, axis=dim), axis, backward)
        block = jnp.concatenate([low, block, high], axis=dim)
    return block


def modulate(rows, norm_gain, scale, shift):
    values = rows.astype(jnp.float32)
    normed = values * lax.rsqrt(jnp.mean(values * values, axis=-1, keepdims=True) + EPS)
    return (normed * norm_gain.astype(jnp.float32) * (1.0 + scale) + shift).astype(jnp.bfloat16)


def project_heads(hidden, weight, gain):
    raw = jnp.dot(hidden, weight, preferred_element_type=jnp.float32)
    split = raw.reshape(hidden.shape[0], -1, HEAD_DIM)
    if gain is None:
        return split.astype(jnp.bfloat16)
    normed = split * lax.rsqrt(jnp.mean(split * split, axis=-1, keepdims=True) + EPS)
    return (normed * gain.astype(jnp.float32)).astype(jnp.bfloat16)


def body(
    latent,
    context,
    cond,
    cond_ctx,
    shift_weight,
    scale_weight,
    gate_weight,
    norm_gain,
    query_weight,
    key_weight,
    value_weight,
    query_gain,
    key_gain,
    offset_bias,
    out_weight,
):
    col_width = shift_weight.shape[1]
    tp_offset = lax.axis_index("tp") * col_width
    act = jax.nn.silu(cond.astype(jnp.float32)).astype(jnp.bfloat16)
    act_ctx = jax.nn.silu(cond_ctx.astype(jnp.float32)).astype(jnp.bfloat16)
    acts = jnp.stack([act, act_ctx])
    terms = jnp.concatenate(
        [
            jnp.dot(acts, shift_weight, preferred_element_type=jnp.float32),
            jnp.dot(acts, scale_weight, preferred_element_type=jnp.float32),
            jnp.dot(acts[:1], gate_weight, preferred_element_type=jnp.float32),
        ],
        axis=0,
    )
    summed = one_axis_at_a_time(terms, SP)
    full = collect(summed, "tp", 1)
    shift, shift_ctx, scale, scale_ctx, gate = (full[0], full[1], full[2], full[3], full[4])
    heads_dev = offset_bias.shape[0]
    lane = heads_dev * HEAD_DIM
    hidden_ctx = modulate(context, norm_gain, scale_ctx, shift_ctx)
    own_keys = project_heads(hidden_ctx, key_weight, key_gain).reshape(context.shape[0], lane)
    own_values = project_heads(hidden_ctx, value_weight, None).reshape(context.shape[0], lane)
    ctx_keys, ctx_values = side_by_side((own_keys, own_values), SP, 0, 1)
    ctx_keys = ctx_keys.reshape(-1, heads_dev, HEAD_DIM)
    ctx_values = ctx_values.reshape(-1, heads_dev, HEAD_DIM)
    hidden = modulate(latent, norm_gain, scale, shift)
    queries = project_heads(hidden, query_weight, query_gain)
    keys = project_heads(hidden, key_weight, key_gain)
    values = project_heads(hidden, value_weight, None)
    rows_dev = latent.shape[0] // GRID_W
    reach = WIN_ROWS // 2
    grid_kv = jnp.stack(
        [keys.reshape(rows_dev, GRID_W, lane), values.reshape(rows_dev, GRID_W, lane)], axis=1
    )
    padded = padded_2(grid_kv, ((SP, 0),), reach)
    total_rows = rows_dev * lax.axis_size(SP)
    base = lax.axis_index(SP) * rows_dev
    local_rows = base + jnp.arange(rows_dev, dtype=jnp.int32)
    first = jnp.clip(local_rows - reach, 0, total_rows - WIN_ROWS)
    window_rows = jnp.arange(WIN_ROWS, dtype=jnp.int32)
    band_index = (first - base + reach)[:, None] + window_rows[None, :]
    band = jnp.take(padded, band_index, axis=0)
    n_blocks = GRID_W // WIN_COLS
    span = 2 * WIN_COLS
    starts = [
        min(max(block * WIN_COLS - WIN_COLS // 2, 0), GRID_W - span) for block in range(n_blocks)
    ]
    blocked = jnp.stack([band[:, :, :, begin : begin + span] for begin in starts], axis=3)
    blocked = blocked.reshape(rows_dev, WIN_ROWS, 2, n_blocks, span, heads_dev, HEAD_DIM)
    key_blocks = blocked[:, :, 0]
    value_blocks = blocked[:, :, 1]
    query_col = np.arange(n_blocks)[:, None, None] * WIN_COLS + np.arange(WIN_COLS)[None, :, None]
    key_col = np.array(starts)[:, None, None] + np.arange(span)[None, None, :]
    window_first = np.clip(query_col - WIN_COLS // 2, 0, GRID_W - WIN_COLS)
    inside = (key_col >= window_first) & (key_col < window_first + WIN_COLS)
    col_offset = np.clip(key_col - query_col + WIN_COLS - 1, 0, 2 * WIN_COLS - 2)
    col_onehot = (col_offset[..., None] == np.arange(2 * WIN_COLS - 1)).astype(np.float32)
    row_offset = first[:, None] + window_rows[None, :] - local_rows[:, None] + WIN_ROWS - 1
    row_onehot = (row_offset[..., None] == jnp.arange(2 * WIN_ROWS - 1, dtype=jnp.int32)).astype(
        jnp.float32
    )
    by_col = jnp.einsum(
        "hxc,bqkc->hxbqk", offset_bias, jnp.asarray(col_onehot), precision=lax.Precision.HIGHEST
    )
    bias = jnp.einsum("rjx,hxbqk->rhbqjk", row_onehot, by_col, precision=lax.Precision.HIGHEST)
    factor = HEAD_DIM ** (-0.5)
    grid_q = queries.reshape(rows_dev, n_blocks, WIN_COLS, heads_dev, HEAD_DIM)
    local_scores = (
        jnp.einsum("rbqhd,rjbkhd->rhbqjk", grid_q, key_blocks, preferred_element_type=jnp.float32)
        * factor
    )
    local_scores = jnp.where(jnp.asarray(inside)[:, :, None, :], local_scores + bias, -jnp.inf)
    band_len = WIN_ROWS * span
    local_scores = local_scores.reshape(rows_dev, heads_dev, n_blocks, WIN_COLS, band_len)
    ctx_scores = (
        jnp.einsum("rbqhd,chd->rhbqc", grid_q, ctx_keys, preferred_element_type=jnp.float32)
        * factor
    )
    scores = jnp.concatenate([local_scores, ctx_scores], axis=-1)
    top = jnp.max(scores, axis=-1, keepdims=True)
    expd = jnp.exp(scores - top)
    weights = (expd / jnp.sum(expd, axis=-1, keepdims=True)).astype(jnp.bfloat16)
    local_w = weights[..., :band_len].reshape(
        rows_dev, heads_dev, n_blocks, WIN_COLS, WIN_ROWS, span
    )
    mixed = jnp.einsum(
        "rhbqjk,rjbkhd->rbqhd", local_w, value_blocks, preferred_element_type=jnp.float32
    )
    mixed = mixed + jnp.einsum(
        "rhbqc,chd->rbqhd", weights[..., band_len:], ctx_values, preferred_element_type=jnp.float32
    )
    mixed = mixed.astype(jnp.bfloat16).reshape(latent.shape[0], lane)
    projected = jnp.dot(collect(mixed, "tp", 1), out_weight, preferred_element_type=jnp.float32)
    own_cols = lax.dynamic_slice_in_dim(latent, tp_offset, col_width, 1).astype(jnp.float32)
    gate_cols = lax.dynamic_slice_in_dim(gate, tp_offset, col_width, 0)
    return (own_cols + gate_cols[None, :] * projected).astype(jnp.bfloat16)


def solution(mesh):
    split = Mesh(mesh.devices.reshape(8, 8, mesh.shape["tp"]), ("sp_0", "sp_1", "tp"))
    placed = (
        P(SP, None),
        P(SP, None),
        P(SP),
        P(SP),
        P(SP, "tp"),
        P(SP, "tp"),
        P(SP, "tp"),
        P(),
        P(None, "tp"),
        P(None, "tp"),
        P(None, "tp"),
        P(),
        P(),
        P("tp", None, None),
        P(None, "tp"),
    )
    return jax.shard_map(body, mesh=split, in_specs=placed, out_specs=P(SP, "tp"), check_vma=False)
```

profile of v0, /device:TPU:1, one launch (start us, length us, event | category | flops | bytes accessed | tf_op | source)
XLA Modules:
  0.0 121.4 jit_solution(677514866326986524)
XLA Ops:
  0.0 0.8 convert_bitcast_fusion
  0.8 0.8 fusion.42
  1.7 0.8 fusion.41
  2.5 0.9 fusion.38
  3.4 20.5 %psum.14 = f32[5,256]{1,0:T(8,128)S(1)} all-reduce(f32[5,256]{1,0:T(8,128)S(1)} %pad_maximum_fusion.2), channel_id=1, replica_groups=mesh['sp_0'=8,'sp_1'=8,'tp'=8] {'sp_0'}, use_global_device_ids=true, to_apply=%region_0.1 | all-reduce | flops 1280 | bytes 10240 | tf_op jit(solution)/shard_map/psum | solution.py:18
  23.9 14.1 %psum.15 = f32[5,256]{1,0:T(8,128)S(1)} all-reduce(f32[5,256]{1,0:T(8,128)S(1)} %psum.14), channel_id=1, replica_groups=mesh['sp_0'=8,'sp_1'=8,'tp'=8] {'sp_1'}, use_global_device_ids=true, to_apply=%region_1.2 | all-reduce | flops 1280 | bytes 10240 | tf_op jit(solution)/shard_map/psum | solution.py:18
  38.0 0.6 broadcast_in_dim.24
  38.6 12.5 %all-to-all-start = ((f32[8,5,256]{2,1,0:T(8,128)}), f32[8,5,256]{2,1,0:T(8,128)S(1)}, u32[]{:S(2)}, u32[]{:S(2)}) async-start(f32[8,5,256]{2,1,0:T(8,128)} %broadcast_in_dim.24), calls=%async_computation | async-start | bytes 131072 | tf_op jit(solution)/shard_map/all_to_all | solution.py:30
  51.3 1.5 %fusion = f32[256]{0:T(256)S(1)} fusion(bf16[256,2048]{1,0:T(8,128)(2,1)} %param.17), kind=kLoop, calls=%fused_computation.3 | loop fusion | flops 1572608 | bytes 1049600 | tf_op jit(solution)/shard_map/reduce_sum | solution.py:59
  52.9 0.9 fusion.25
  53.9 5.6 %convolution_bitcast_fusion = f32[2,15,4,16,32,1]{4,1,5,3,2,0:T(8,128)S(1)} fusion(f32[4,16,32,31,1]{3,2,1,0,4:T(8,128)S(1)} %copy-done.5, f32[2,15,31,1,1]{2,0,1,4,3:T(2,128)} %bitcast.131), kind=kOutput, calls=%fused_computation.20 | convolution fusion | flops 22855680 | bytes 503432 | tf_op jit(solution)/shard_map/hxc,bqkc->hxbqk/dot_general | solution.py:149
  59.5 2.3 %fusion.32 = f32[2,4,16,32,4,8]{3,5,4,2,1,0:T(8,128)} fusion(f32[2,15,4,16,32,1]{4,1,5,3,2,0:T(8,128)S(1)} %convolution_bitcast_fusion, s32[4,8]{1,0:T(4,128)S(1)} %subtract_add_fusion), kind=kOutput, calls=%fused_computation.59 | convolution fusion | flops 23593440 | bytes 770176 | tf_op jit(solution)/shard_map/rjx,hxbqk->rhbqjk/dot_general | solution.py:152
  64.2 1.8 %collective-permute-start = (bf16[4,2,64,128]{3,2,0,1:T(8,128)(2,1)S(1)}, bf16[4,2,64,128]{3,2,0,1:T(8,128)(2,1)S(1)}, u32[]{:S(2)}, u32[]{:S(2)}) collective-permute-start(bf16[4,2,64,128]{3,2,0,1:T(8,128)(2,1)S(1)} %pad_maximum_fusion.1), channel_id=1, source_target_pairs={{0,8},{8,16},{16,24},{24,32},{32,40},{40,48},{48,56},{56,64},{64,7... | collective-permute-start | bytes 393224 | tf_op jit(solution)/shard_map/ppermute | solution.py:49
  66.0 1.3 %collective-permute-start.1 = (bf16[4,2,64,128]{3,2,0,1:T(8,128)(2,1)S(1)}, bf16[4,2,64,128]{3,2,0,1:T(8,128)(2,1)S(1)}, u32[]{:S(2)}, u32[]{:S(2)}) collective-permute-start(bf16[4,2,64,128]{3,2,0,1:T(8,128)(2,1)S(1)} %pad_maximum_fusion.1), channel_id=1, source_target_pairs={{8,0},{16,8},{24,16},{32,24},{40,32},{48,40},{56,48},{64,56},{72,6... | collective-permute-start | bytes 393224 | tf_op jit(solution)/shard_map/ppermute | solution.py:52
  69.1 0.7 broadcast_in_dim.29
  69.8 9.8 %all-to-all-start.1 = ((bf16[64,8,256]{2,1,0:T(8,128)(2,1)}), bf16[64,8,256]{2,1,0:T(8,128)(2,1)}, u32[]{:S(2)}, u32[]{:S(2)}) async-start(bf16[64,8,256]{2,1,0:T(8,128)(2,1)} %broadcast_in_dim.29), calls=%async_computation.1 | async-start | bytes 524288 | tf_op jit(solution)/shard_map/all_to_all | solution.py:30
  79.7 0.7 gather_fusion
  80.6 1.4 %fusion.46 = (bf16[4,8,2,32,128]{4,3,2,1,0:T(8,128)(2,1)S(1)}, bf16[4,8,2,32,128]{4,3,2,1,0:T(8,128)(2,1)}, bf16[4,8,2,32,128]{4,3,2,1,0:T(8,128)(2,1)S(1)}, bf16[4,8,2,32,128]{4,3,2,1,0:T(8,128)(2,1)S(1)}) fusion(bf16[4,8,2,64,128]{4,3,2,1,0:T(8,128)(2,1)S(1)} %broadcast_select_fusion), kind=kLoop, calls=%fused_computation.92 | loop fusion | bytes 4194304 | tf_op jit(solution)/shard_map/slice | solution.py:135
  82.4 1.2 copy_dynamic-update-slice_fusion.3
  84.1 2.5 %stack.33 = bf16[4,8,2,1,32,2,64]{6,5,4,2,1,0,3:T(2,128)(2,1)S(1)} reshape(bf16[4,8,2,32,128]{4,3,2,1,0:T(8,128)(2,1)} %get-tuple-element.6) | data formatting | bytes 1048576 | tf_op jit(solution)/shard_map/stack | solution.py:135
  86.5 1.4 %stack.34 = bf16[4,8,2,1,32,2,64]{6,5,4,2,1,0,3:T(2,128)(2,1)} reshape(bf16[4,8,2,32,128]{4,3,2,1,0:T(8,128)(2,1)S(1)} %get-tuple-element.5) | data formatting | bytes 1048576 | tf_op jit(solution)/shard_map/stack | solution.py:135
  87.9 1.2 copy_dynamic-update-slice_fusion.2
  89.1 1.2 copy_dynamic-update-slice_fusion.1
  90.3 1.2 copy_dynamic-update-slice_fusion
  91.5 4.5 %fusion.51 = (f32[4,2,4,16]{3,2,1,0:T(4,128)S(1)}, f32[4,2,4,16,8,32]{5,3,4,2,1,0:T(8,128)S(1)}) fusion(f32[2,4,16,32,4,8]{3,5,4,2,1,0:T(8,128)S(1)} %copy-done.1, bf16[4,8,2,4,32,2,64]{6,4,1,3,5,0,2:T(8,128)(2,1)} %copy_dynamic-update-slice_fusion, pred[4,16,32]{2,1,0:T(8,128)(4,1)S(1)} %copy-done.8, f32[64]{0:T(128)S(1)} %convert_element_type.95, ...), kind=kOutput, calls=%fused_computation.97 | convolution fusion | flops 17399296 | bytes 3283200 | tf_op jit(solution)/shard_map/rbqhd,rjbkhd->rhbqjk/dot_general | solution.py:156
  96.1 0.9 copy.124
  97.6 1.0 fusion.47
  100.4 2.5 %fusion.12 = f32[4,4,16,2,64]{4,2,3,1,0:T(8,128)S(1)} fusion(bf16[4,2,4,16,8,32]{5,4,3,2,0,1:T(8,128)(2,1)S(1)} %reshape.279, bf16[4,8,2,4,32,2,64]{6,4,1,3,5,0,2:T(8,128)(2,1)} %copy_dynamic-update-slice_fusion), kind=kOutput, calls=%fused_computation.23 | convolution fusion | flops 16777216 | bytes 2490368 | tf_op jit(solution)/shard_map/rhbqjk,rjbkhd->rbqhd/dot_general | solution.py:173
  103.6 0.8 broadcast_in_dim.30
  104.5 5.6 %all-to-all-start.2 = ((bf16[8,256,128]{1,2,0:T(8,128)(2,1)}), bf16[8,256,128]{1,2,0:T(8,128)(2,1)S(1)}, u32[]{:S(2)}, u32[]{:S(2)}) async-start(bf16[8,256,128]{1,2,0:T(8,128)(2,1)} %broadcast_in_dim.30), calls=%async_computation.2 | async-start | bytes 1048576 | tf_op jit(solution)/shard_map/all_to_all | solution.py:30
  110.2 9.3 %all-to-all-done.2 = bf16[8,256,128]{1,2,0:T(8,128)(2,1)S(1)} async-done(((bf16[8,256,128]{1,2,0:T(8,128)(2,1)}), bf16[8,256,128]{1,2,0:T(8,128)(2,1)S(1)}, u32[]{:S(2)}, u32[]{:S(2)}) %all-to-all-start.2) | async-done | bytes 524320 | tf_op jit(solution)/shard_map/all_to_all | solution.py:30
  119.5 1.9 %fusion.17 = bf16[256,256]{1,0:T(8,128)(2,1)} fusion(bf16[256,1024]{0,1:T(8,128)(2,1)S(1)} %bitcast.121, bf16[1024,256]{1,0:T(8,128)(2,1)S(1)} %copy-done.10, f32[256]{0:T(256)S(1)} %dynamic_slice.7, bf16[256,2048]{1,0:T(8,128)(2,1)} %param.17, s32[]{:T(128)S(6)} %select_n.28), kind=kOutput, calls=%fused_computation.27 | convolution fusion | flops 134479872 | bytes 1311748 | tf_op jit(solution)/shard_map/dot_general | solution.py:180
  (89 shorter events, 8.6 us)
Async XLA Ops:
  0.0 62.5 %copy-start = (bf16[2048,128]{1,0:T(8,128)(2,1)S(1)}, bf16[2048,128]{1,0:T(8,128)(2,1)}, u32[]{:S(2)}) copy-start(bf16[2048,128]{1,0:T(8,128)(2,1)} %param.26) | copy-start | bytes 1572868
  0.0 53.9 %copy-start.5 = (f32[4,16,32,31,1]{3,2,1,0,4:T(8,128)S(1)}, f32[4,16,32,31,1]{3,2,1,0,4:T(8,128)}, u32[]{:S(2)}) copy-start(f32[4,16,32,31,1]{3,2,1,0,4:T(8,128)} %constant.87) | copy-start | bytes 761860
  38.6 23.3 %all-to-all-start = ((f32[8,5,256]{2,1,0:T(8,128)}), f32[8,5,256]{2,1,0:T(8,128)S(1)}, u32[]{:S(2)}, u32[]{:S(2)}) async-start(f32[8,5,256]{2,1,0:T(8,128)} %broadcast_in_dim.24), calls=%async_computation | async-start | bytes 131072 | tf_op jit(solution)/shard_map/all_to_all | solution.py:30
  59.4 2.4 %copy-start.9 = (bf16[2048]{0:T(1024)(128)(2,1)S(1)}, bf16[2048]{0:T(1024)(128)(2,1)}, u32[]{:S(2)}) copy-start(bf16[2048]{0:T(1024)(128)(2,1)} %param.24) | copy-start | bytes 12292
  59.4 2.4 %copy-start.11 = (bf16[64]{0:T(256)(128)(2,1)S(1)}, bf16[64]{0:T(256)(128)(2,1)}, u32[]{:S(2)}) copy-start(bf16[64]{0:T(256)(128)(2,1)} %param.29) | copy-start | bytes 388
  59.5 2.5 %copy-start.12 = (bf16[64]{0:T(256)(128)(2,1)S(1)}, bf16[64]{0:T(256)(128)(2,1)}, u32[]{:S(2)}) copy-start(bf16[64]{0:T(256)(128)(2,1)} %param.28) | copy-start | bytes 388
  59.5 2.5 %copy-start.2 = (bf16[256,2048]{1,0:T(8,128)(2,1)S(1)}, bf16[256,2048]{1,0:T(8,128)(2,1)}, u32[]{:S(2)}) copy-start(bf16[256,2048]{1,0:T(8,128)(2,1)} %param.17) | copy-start | bytes 3145732
  62.5 1.3 %copy-start.4 = (bf16[2048,128]{1,0:T(8,128)(2,1)S(1)}, bf16[2048,128]{1,0:T(8,128)(2,1)}, u32[]{:S(2)}) copy-start(bf16[2048,128]{1,0:T(8,128)(2,1)} %param.27) | copy-start | bytes 1572868
  62.9 4.4 %copy-start.7 = (bf16[8,2048]{1,0:T(8,128)(2,1)S(1)}, bf16[8,2048]{1,0:T(8,128)(2,1)}, u32[]{:S(2)}) copy-start(bf16[8,2048]{1,0:T(8,128)(2,1)} %param.18) | copy-start | bytes 98308
  63.2 4.6 %copy-start.6 = (bf16[2048,128]{1,0:T(8,128)(2,1)S(1)}, bf16[2048,128]{1,0:T(8,128)(2,1)}, u32[]{:S(2)}) copy-start(bf16[2048,128]{1,0:T(8,128)(2,1)} %param.25) | copy-start | bytes 1572868
  64.2 15.4 %collective-permute-start = (bf16[4,2,64,128]{3,2,0,1:T(8,128)(2,1)S(1)}, bf16[4,2,64,128]{3,2,0,1:T(8,128)(2,1)S(1)}, u32[]{:S(2)}, u32[]{:S(2)}) collective-permute-start(bf16[4,2,64,128]{3,2,0,1:T(8,128)(2,1)S(1)} %pad_maximum_fusion.1), channel_id=1, source_target_pairs={{0,8},{8,16},{16,24},{24,32},{32,40},{40,48},{48,56},{56,64},{64,7... | collective-permute-start | bytes 393224 | tf_op jit(solution)/shard_map/ppermute | solution.py:49
  66.0 13.6 %collective-permute-start.1 = (bf16[4,2,64,128]{3,2,0,1:T(8,128)(2,1)S(1)}, bf16[4,2,64,128]{3,2,0,1:T(8,128)(2,1)S(1)}, u32[]{:S(2)}, u32[]{:S(2)}) collective-permute-start(bf16[4,2,64,128]{3,2,0,1:T(8,128)(2,1)S(1)} %pad_maximum_fusion.1), channel_id=1, source_target_pairs={{8,0},{16,8},{24,16},{32,24},{40,32},{48,40},{56,48},{64,56},{72,6... | collective-permute-start | bytes 393224 | tf_op jit(solution)/shard_map/ppermute | solution.py:52
  69.8 27.7 %all-to-all-start.1 = ((bf16[64,8,256]{2,1,0:T(8,128)(2,1)}), bf16[64,8,256]{2,1,0:T(8,128)(2,1)}, u32[]{:S(2)}, u32[]{:S(2)}) async-start(bf16[64,8,256]{2,1,0:T(8,128)(2,1)} %broadcast_in_dim.29), calls=%async_computation.1 | async-start | bytes 524288 | tf_op jit(solution)/shard_map/all_to_all | solution.py:30
  87.9 2.4 %copy-start.3 = (bf16[4,8,2,1,32,2,64]{6,5,4,2,1,0,3:T(2,128)(2,1)S(1)}, bf16[4,8,2,1,32,2,64]{6,5,4,2,1,0,3:T(2,128)(2,1)}, u32[]{:S(2)}) copy-start(bf16[4,8,2,1,32,2,64]{6,5,4,2,1,0,3:T(2,128)(2,1)} %stack.34) | copy-start | bytes 1572868
  89.1 2.4 %copy-start.1 = (f32[2,4,16,32,4,8]{3,5,4,2,1,0:T(8,128)S(1)}, f32[2,4,16,32,4,8]{3,5,4,2,1,0:T(8,128)}, u32[]{:S(2)}) copy-start(f32[2,4,16,32,4,8]{3,5,4,2,1,0:T(8,128)} %fusion.32) | copy-start | bytes 1572868
  89.1 2.4 %copy-start.8 = (pred[4,16,32]{2,1,0:T(8,128)(4,1)S(1)}, pred[4,16,32]{2,1,0:T(8,128)(4,1)}, u32[]{:S(2)}) copy-start(pred[4,16,32]{2,1,0:T(8,128)(4,1)} %constant.79.clone) | copy-start | bytes 6148
  102.9 16.6 %copy-start.10 = (bf16[1024,256]{1,0:T(8,128)(2,1)S(1)}, bf16[1024,256]{1,0:T(8,128)(2,1)}, u32[]{:S(2)}) copy-start(bf16[1024,256]{1,0:T(8,128)(2,1)} %param.31) | copy-start | bytes 1572868
  104.5 15.0 %all-to-all-start.2 = ((bf16[8,256,128]{1,2,0:T(8,128)(2,1)}), bf16[8,256,128]{1,2,0:T(8,128)(2,1)S(1)}, u32[]{:S(2)}, u32[]{:S(2)}) async-start(bf16[8,256,128]{1,2,0:T(8,128)(2,1)} %broadcast_in_dim.30), calls=%async_computation.2 | async-start | bytes 1048576 | tf_op jit(solution)/shard_map/all_to_all | solution.py:30
where the time goes:
time: 122 us; the launch traced here: 121 us
  blocking collectives  34.6 us (28%)
  starting transfers between devices  31 us (25%)
  matrix products  21.9 us (18%)
  local copies, waits for them, and re-layouts  18.9 us (15%)
  waiting for transfers between devices  9.29 us (8%)
  other arithmetic  5.2 us (4%)
    psum x2, blocking collectives, one_axis_at_a_time(): x = lax.psum(x, axis)  34.6 us
    all_to_all x3, starting transfers between devices, sent_to_all(): return lax.all_to_all(copies, axis, split_axis=0, concat_axis=0, tiled=True)  27.9 us
    all_to_all x3, waiting for transfers between devices, sent_to_all(): return lax.all_to_all(copies, axis, split_axis=0, concat_axis=0, tiled=True)  9.28 us
    another operation x5, local copies, waits for them, and re-layouts, body(): jnp.stack([band[:, :, :, begin:begin + span] for begin in starts], axis=3)  5.84 us
    dot_general x1, matrix products, body(): jnp.einsum('hxc,bqkc->hxbqk', offset_bias, jnp.asarray(col_onehot), preci...  5.56 us
    dot_general x1, matrix products, body(): jnp.einsum('rbqhd,rjbkhd->rhbqjk', grid_q, key_blocks, preferred_element_...  4.53 us
    unnamed x29, local copies, waits for them, and re-layouts  3.67 us
    dot_general x1, matrix products, body(): jnp.einsum('rhbqjk,rjbkhd->rbqhd', local_w, value_blocks, preferred_eleme...  2.47 us
  transfers between devices with their start and end apart: 5, of which 1 were waited for; matrix products, arithmetic and copies ran while one was open for 26% of the time, Pallas kernels for 0%

commit v1 on v0

--- a/solution.py
+++ b/solution.py
@@ -15,7 +15,7 @@
 
 def one_axis_at_a_time(x, axes):
     for axis in axes:
-        x = lax.psum(x, axis)
+        x = jax.lax.all_gather(x, axis_name=axis).sum(axis=0)
     return x
 
 

time: 122 us -> 140 us (1.15)
  blocking collectives: 34.6 us -> 45.8 us
  starting transfers between devices: 31 us -> 38.1 us
    all_gather x0 -> x2, blocking collectives: none -> 45.8 us  [one_axis_at_a_time(): x = jax.lax.all_gather(x, axis_name=axis).sum(axis=0)]
    psum x2 -> x0, blocking collectives: 34.6 us -> none  [one_axis_at_a_time(): x = lax.psum(x, axis)]
    all_to_all x3, starting transfers between devices: 27.9 us -> 34.5 us  [sent_to_all(): return lax.all_to_all(copies, axis, split_axis=0, concat_axis=0, tiled=True)]
  transfers between devices with their start and end apart: 5 -> 5, of which waited for: 1 -> 1; matrix products, arithmetic and copies ran while one was open for 26% -> 22% of each run, Pallas kernels for 0% -> 0%
where the time goes in v1:
time: 140 us
  blocking collectives  45.8 us (33%)
  starting transfers between devices  38.1 us (27%)
  matrix products  21.9 us (16%)
  local copies, waits for them, and re-layouts  18.9 us (13%)
  waiting for transfers between devices  9.29 us (7%)
  other arithmetic  5.23 us (4%)
    all_gather x2, blocking collectives, one_axis_at_a_time(): x = jax.lax.all_gather(x, axis_name=axis).sum(axis=0)  45.8 us
    all_to_all x3, starting transfers between devices, sent_to_all(): return lax.all_to_all(copies, axis, split_axis=0, concat_axis=0, tiled=True)  34.5 us
    all_to_all x3, waiting for transfers between devices, sent_to_all(): return lax.all_to_all(copies, axis, split_axis=0, concat_axis=0, tiled=True)  9.28 us
    another operation x5, local copies, waits for them, and re-layouts, body(): jnp.stack([band[:, :, :, begin:begin + span] for begin in starts], axis=3)  5.84 us
    dot_general x1, matrix products, body(): jnp.einsum('hxc,bqkc->hxbqk', offset_bias, jnp.asarray(col_onehot), preci...  5.56 us
    dot_general x1, matrix products, body(): jnp.einsum('rbqhd,rjbkhd->rhbqjk', grid_q, key_blocks, preferred_element_...  4.53 us
    unnamed x29, local copies, waits for them, and re-layouts  3.67 us
  transfers between devices with their start and end apart: 5, of which 1 were waited for; matrix products, arithmetic and copies ran while one was open for 22% of the time, Pallas kernels for 0%

profile of v1, /device:TPU:1, one launch (start us, length us, event | category | flops | bytes accessed | tf_op | source)
XLA Modules:
  0.0 139.6 jit_solution(13964885250409873426)
XLA Ops:
  0.0 0.8 convert_bitcast_fusion
  0.8 0.8 fusion.42
  1.7 0.8 fusion.41
  2.5 0.9 fusion.38
  3.4 25.7 %all-gather.2 = f32[8,5,256]{2,1,0:T(8,128)S(1)} all-gather(f32[1,5,256]{2,1,0:T(8,128)S(1)} %maximum_bitcast_fusion), channel_id=2, replica_groups=mesh['sp_0'=8,'sp_1'=8,'tp'=8] {'sp_0'}, dimensions={0}, use_global_device_ids=true | all-gather | bytes 46080 | tf_op jit(solution)/shard_map/all_gather | solution.py:18
  29.1 20.1 %all-gather.3 = f32[8,5,256]{2,1,0:T(8,128)S(1)} all-gather(f32[1,5,256]{2,1,0:T(8,128)S(1)} %bitcast.134), channel_id=3, replica_groups=mesh['sp_0'=8,'sp_1'=8,'tp'=8] {'sp_1'}, dimensions={0}, use_global_device_ids=true | all-gather | bytes 46080 | tf_op jit(solution)/shard_map/all_gather | solution.py:18
  49.2 0.6 broadcast_in_dim.24
  49.8 17.1 %all-to-all-start = ((f32[8,5,256]{2,1,0:T(8,128)}), f32[8,5,256]{2,1,0:T(8,128)S(1)}, u32[]{:S(2)}, u32[]{:S(2)}) async-start(f32[8,5,256]{2,1,0:T(8,128)} %broadcast_in_dim.24), calls=%async_computation | async-start | bytes 131072 | tf_op jit(solution)/shard_map/all_to_all | solution.py:30
  67.1 1.5 %fusion = f32[256]{0:T(256)S(1)} fusion(bf16[256,2048]{1,0:T(8,128)(2,1)} %param.17), kind=kLoop, calls=%fused_computation.3 | loop fusion | flops 1572608 | bytes 1049600 | tf_op jit(solution)/shard_map/reduce_sum | solution.py:59
  68.7 0.9 fusion.25
  69.7 5.6 %convolution_bitcast_fusion = f32[2,15,4,16,32,1]{4,1,5,3,2,0:T(8,128)S(1)} fusion(f32[4,16,32,31,1]{3,2,1,0,4:T(8,128)S(1)} %copy-done.5, f32[2,15,31,1,1]{2,0,1,4,3:T(2,128)} %bitcast.135), kind=kOutput, calls=%fused_computation.20 | convolution fusion | flops 22855680 | bytes 503432 | tf_op jit(solution)/shard_map/hxc,bqkc->hxbqk/dot_general | solution.py:149
  75.3 2.3 %fusion.32 = f32[2,4,16,32,4,8]{3,5,4,2,1,0:T(8,128)} fusion(f32[2,15,4,16,32,1]{4,1,5,3,2,0:T(8,128)S(1)} %convolution_bitcast_fusion, s32[4,8]{1,0:T(4,128)S(1)} %subtract_add_fusion), kind=kOutput, calls=%fused_computation.59 | convolution fusion | flops 23593440 | bytes 770176 | tf_op jit(solution)/shard_map/rjx,hxbqk->rhbqjk/dot_general | solution.py:152
  80.1 2.3 %collective-permute-start = (bf16[4,2,64,128]{3,2,0,1:T(8,128)(2,1)S(1)}, bf16[4,2,64,128]{3,2,0,1:T(8,128)(2,1)S(1)}, u32[]{:S(2)}, u32[]{:S(2)}) collective-permute-start(bf16[4,2,64,128]{3,2,0,1:T(8,128)(2,1)S(1)} %pad_maximum_fusion.1), channel_id=1, source_target_pairs={{0,8},{8,16},{16,24},{24,32},{32,40},{40,48},{48,56},{56,64},{64,7... | collective-permute-start | bytes 393224 | tf_op jit(solution)/shard_map/ppermute | solution.py:49
  82.4 1.3 collective-permute-start.1
  85.5 0.7 broadcast_in_dim.29
  86.2 11.7 %all-to-all-start.1 = ((bf16[64,8,256]{2,1,0:T(8,128)(2,1)}), bf16[64,8,256]{2,1,0:T(8,128)(2,1)}, u32[]{:S(2)}, u32[]{:S(2)}) async-start(bf16[64,8,256]{2,1,0:T(8,128)(2,1)} %broadcast_in_dim.29), calls=%async_computation.1 | async-start | bytes 524288 | tf_op jit(solution)/shard_map/all_to_all | solution.py:30
  98.0 0.7 gather_fusion
  98.9 1.4 %fusion.46 = (bf16[4,8,2,32,128]{4,3,2,1,0:T(8,128)(2,1)S(1)}, bf16[4,8,2,32,128]{4,3,2,1,0:T(8,128)(2,1)}, bf16[4,8,2,32,128]{4,3,2,1,0:T(8,128)(2,1)S(1)}, bf16[4,8,2,32,128]{4,3,2,1,0:T(8,128)(2,1)S(1)}) fusion(bf16[4,8,2,64,128]{4,3,2,1,0:T(8,128)(2,1)S(1)} %broadcast_select_fusion), kind=kLoop, calls=%fused_computation.92 | loop fusion | bytes 4194304 | tf_op jit(solution)/shard_map/slice | solution.py:135
  100.7 1.2 copy_dynamic-update-slice_fusion.3
  102.3 2.5 %stack.33 = bf16[4,8,2,1,32,2,64]{6,5,4,2,1,0,3:T(2,128)(2,1)S(1)} reshape(bf16[4,8,2,32,128]{4,3,2,1,0:T(8,128)(2,1)} %get-tuple-element.6) | data formatting | bytes 1048576 | tf_op jit(solution)/shard_map/stack | solution.py:135
  104.8 1.4 %stack.34 = bf16[4,8,2,1,32,2,64]{6,5,4,2,1,0,3:T(2,128)(2,1)} reshape(bf16[4,8,2,32,128]{4,3,2,1,0:T(8,128)(2,1)S(1)} %get-tuple-element.5) | data formatting | bytes 1048576 | tf_op jit(solution)/shard_map/stack | solution.py:135
  106.2 1.2 copy_dynamic-update-slice_fusion.2
  107.4 1.2 copy_dynamic-update-slice_fusion.1
  108.6 1.2 copy_dynamic-update-slice_fusion
  109.8 4.5 %fusion.51 = (f32[4,2,4,16]{3,2,1,0:T(4,128)S(1)}, f32[4,2,4,16,8,32]{5,3,4,2,1,0:T(8,128)S(1)}) fusion(f32[2,4,16,32,4,8]{3,5,4,2,1,0:T(8,128)S(1)} %copy-done.1, bf16[4,8,2,4,32,2,64]{6,4,1,3,5,0,2:T(8,128)(2,1)} %copy_dynamic-update-slice_fusion, pred[4,16,32]{2,1,0:T(8,128)(4,1)S(1)} %copy-done.8, f32[64]{0:T(128)S(1)} %convert_element_type.95, ...), kind=kOutput, calls=%fused_computation.97 | convolution fusion | flops 17399296 | bytes 3283200 | tf_op jit(solution)/shard_map/rbqhd,rjbkhd->rhbqjk/dot_general | solution.py:156
  114.3 0.9 copy.124
  115.8 1.0 fusion.47
  118.7 2.5 %fusion.12 = f32[4,4,16,2,64]{4,2,3,1,0:T(8,128)S(1)} fusion(bf16[4,2,4,16,8,32]{5,4,3,2,0,1:T(8,128)(2,1)S(1)} %reshape.279, bf16[4,8,2,4,32,2,64]{6,4,1,3,5,0,2:T(8,128)(2,1)} %copy_dynamic-update-slice_fusion), kind=kOutput, calls=%fused_computation.23 | convolution fusion | flops 16777216 | bytes 2490368 | tf_op jit(solution)/shard_map/rhbqjk,rjbkhd->rbqhd/dot_general | solution.py:173
  121.9 0.8 broadcast_in_dim.30
  122.7 5.7 %all-to-all-start.2 = ((bf16[8,256,128]{1,2,0:T(8,128)(2,1)}), bf16[8,256,128]{1,2,0:T(8,128)(2,1)S(1)}, u32[]{:S(2)}, u32[]{:S(2)}) async-start(bf16[8,256,128]{1,2,0:T(8,128)(2,1)} %broadcast_in_dim.30), calls=%async_computation.2 | async-start | bytes 1048576 | tf_op jit(solution)/shard_map/all_to_all | solution.py:30
  128.4 9.3 %all-to-all-done.2 = bf16[8,256,128]{1,2,0:T(8,128)(2,1)S(1)} async-done(((bf16[8,256,128]{1,2,0:T(8,128)(2,1)}), bf16[8,256,128]{1,2,0:T(8,128)(2,1)S(1)}, u32[]{:S(2)}, u32[]{:S(2)}) %all-to-all-start.2) | async-done | bytes 524320 | tf_op jit(solution)/shard_map/all_to_all | solution.py:30
  137.7 1.9 %fusion.17 = bf16[256,256]{1,0:T(8,128)(2,1)} fusion(bf16[256,1024]{0,1:T(8,128)(2,1)S(1)} %bitcast.124, bf16[1024,256]{1,0:T(8,128)(2,1)S(1)} %copy-done.10, f32[256]{0:T(256)S(1)} %dynamic_slice.7, bf16[256,2048]{1,0:T(8,128)(2,1)} %param.17, s32[]{:T(128)S(6)} %select_n.28), kind=kOutput, calls=%fused_computation.27 | convolution fusion | flops 134479872 | bytes 1311748 | tf_op jit(solution)/shard_map/dot_general | solution.py:180
  (91 shorter events, 8.6 us)
Async XLA Ops:
  0.0 78.3 %copy-start = (bf16[2048,128]{1,0:T(8,128)(2,1)S(1)}, bf16[2048,128]{1,0:T(8,128)(2,1)}, u32[]{:S(2)}) copy-start(bf16[2048,128]{1,0:T(8,128)(2,1)} %param.26) | copy-start | bytes 1572868
  0.0 69.7 %copy-start.5 = (f32[4,16,32,31,1]{3,2,1,0,4:T(8,128)S(1)}, f32[4,16,32,31,1]{3,2,1,0,4:T(8,128)}, u32[]{:S(2)}) copy-start(f32[4,16,32,31,1]{3,2,1,0,4:T(8,128)} %constant.87) | copy-start | bytes 761860
  49.8 27.9 %all-to-all-start = ((f32[8,5,256]{2,1,0:T(8,128)}), f32[8,5,256]{2,1,0:T(8,128)S(1)}, u32[]{:S(2)}, u32[]{:S(2)}) async-start(f32[8,5,256]{2,1,0:T(8,128)} %broadcast_in_dim.24), calls=%async_computation | async-start | bytes 131072 | tf_op jit(solution)/shard_map/all_to_all | solution.py:30
  75.3 2.4 %copy-start.9 = (bf16[2048]{0:T(1024)(128)(2,1)S(1)}, bf16[2048]{0:T(1024)(128)(2,1)}, u32[]{:S(2)}) copy-start(bf16[2048]{0:T(1024)(128)(2,1)} %param.24) | copy-start | bytes 12292
  75.3 2.4 %copy-start.11 = (bf16[64]{0:T(256)(128)(2,1)S(1)}, bf16[64]{0:T(256)(128)(2,1)}, u32[]{:S(2)}) copy-start(bf16[64]{0:T(256)(128)(2,1)} %param.29) | copy-start | bytes 388
  75.3 2.5 %copy-start.12 = (bf16[64]{0:T(256)(128)(2,1)S(1)}, bf16[64]{0:T(256)(128)(2,1)}, u32[]{:S(2)}) copy-start(bf16[64]{0:T(256)(128)(2,1)} %param.28) | copy-start | bytes 388
  75.3 2.5 %copy-start.2 = (bf16[256,2048]{1,0:T(8,128)(2,1)S(1)}, bf16[256,2048]{1,0:T(8,128)(2,1)}, u32[]{:S(2)}) copy-start(bf16[256,2048]{1,0:T(8,128)(2,1)} %param.17) | copy-start | bytes 3145732
  78.3 1.3 copy-start.4
  78.8 4.9 %copy-start.7 = (bf16[8,2048]{1,0:T(8,128)(2,1)S(1)}, bf16[8,2048]{1,0:T(8,128)(2,1)}, u32[]{:S(2)}) copy-start(bf16[8,2048]{1,0:T(8,128)(2,1)} %param.18) | copy-start | bytes 98308
  79.1 5.1 %copy-start.6 = (bf16[2048,128]{1,0:T(8,128)(2,1)S(1)}, bf16[2048,128]{1,0:T(8,128)(2,1)}, u32[]{:S(2)}) copy-start(bf16[2048,128]{1,0:T(8,128)(2,1)} %param.25) | copy-start | bytes 1572868
  80.1 17.8 %collective-permute-start = (bf16[4,2,64,128]{3,2,0,1:T(8,128)(2,1)S(1)}, bf16[4,2,64,128]{3,2,0,1:T(8,128)(2,1)S(1)}, u32[]{:S(2)}, u32[]{:S(2)}) collective-permute-start(bf16[4,2,64,128]{3,2,0,1:T(8,128)(2,1)S(1)} %pad_maximum_fusion.1), channel_id=1, source_target_pairs={{0,8},{8,16},{16,24},{24,32},{32,40},{40,48},{48,56},{56,64},{64,7... | collective-permute-start | bytes 393224 | tf_op jit(solution)/shard_map/ppermute | solution.py:49
  82.4 15.5 %collective-permute-start.1 = (bf16[4,2,64,128]{3,2,0,1:T(8,128)(2,1)S(1)}, bf16[4,2,64,128]{3,2,0,1:T(8,128)(2,1)S(1)}, u32[]{:S(2)}, u32[]{:S(2)}) collective-permute-start(bf16[4,2,64,128]{3,2,0,1:T(8,128)(2,1)S(1)} %pad_maximum_fusion.1), channel_id=1, source_target_pairs={{8,0},{16,8},{24,16},{32,24},{40,32},{48,40},{56,48},{64,56},{72,6... | collective-permute-start | bytes 393224 | tf_op jit(solution)/shard_map/ppermute | solution.py:52
  86.2 29.6 %all-to-all-start.1 = ((bf16[64,8,256]{2,1,0:T(8,128)(2,1)}), bf16[64,8,256]{2,1,0:T(8,128)(2,1)}, u32[]{:S(2)}, u32[]{:S(2)}) async-start(bf16[64,8,256]{2,1,0:T(8,128)(2,1)} %broadcast_in_dim.29), calls=%async_computation.1 | async-start | bytes 524288 | tf_op jit(solution)/shard_map/all_to_all | solution.py:30
  106.2 2.4 %copy-start.3 = (bf16[4,8,2,1,32,2,64]{6,5,4,2,1,0,3:T(2,128)(2,1)S(1)}, bf16[4,8,2,1,32,2,64]{6,5,4,2,1,0,3:T(2,128)(2,1)}, u32[]{:S(2)}) copy-start(bf16[4,8,2,1,32,2,64]{6,5,4,2,1,0,3:T(2,128)(2,1)} %stack.34) | copy-start | bytes 1572868
  107.4 2.4 %copy-start.1 = (f32[2,4,16,32,4,8]{3,5,4,2,1,0:T(8,128)S(1)}, f32[2,4,16,32,4,8]{3,5,4,2,1,0:T(8,128)}, u32[]{:S(2)}) copy-start(f32[2,4,16,32,4,8]{3,5,4,2,1,0:T(8,128)} %fusion.32) | copy-start | bytes 1572868
  107.4 2.4 %copy-start.8 = (pred[4,16,32]{2,1,0:T(8,128)(4,1)S(1)}, pred[4,16,32]{2,1,0:T(8,128)(4,1)}, u32[]{:S(2)}) copy-start(pred[4,16,32]{2,1,0:T(8,128)(4,1)} %constant.79.clone) | copy-start | bytes 6148
  121.1 16.6 %copy-start.10 = (bf16[1024,256]{1,0:T(8,128)(2,1)S(1)}, bf16[1024,256]{1,0:T(8,128)(2,1)}, u32[]{:S(2)}) copy-start(bf16[1024,256]{1,0:T(8,128)(2,1)} %param.31) | copy-start | bytes 1572868
  122.7 15.0 %all-to-all-start.2 = ((bf16[8,256,128]{1,2,0:T(8,128)(2,1)}), bf16[8,256,128]{1,2,0:T(8,128)(2,1)S(1)}, u32[]{:S(2)}, u32[]{:S(2)}) async-start(bf16[8,256,128]{1,2,0:T(8,128)(2,1)} %broadcast_in_dim.30), calls=%async_computation.2 | async-start | bytes 1048576 | tf_op jit(solution)/shard_map/all_to_all | solution.py:30
